TPU v7x, 512 devices: a 8x2x16 block of a 8x8x16 slice. The times are simulated.
512 devices in a mesh: grp: 2 (over y), dp: 8 (over x), kv: 16 (over z), tp: 2 (over core).
Axes of the slice: x: 8, y: 2, z: 16, core: 2. Of those that a mesh axis runs over, the one named last changes fastest.
The devices are a block of a 8x8x16 slice.
Arguments:
- tokens: bfloat16 [1024, 4, 4096], P(('grp', 'dp'), None, 'kv'), parts along dimension 0, may hold values from -6 to 6
- w_query: bfloat16 [4096, 2048], P('kv', 'tp'), may hold values from -0.09375 to 0.09375
- w_forget: bfloat16 [4096, 2048], P('kv', 'tp'), may hold values from -0.09375 to 0.09375
- w_input: bfloat16 [4096, 2048], P('kv', 'tp'), may hold values from -0.09375 to 0.09375
- w_gate: bfloat16 [4096, 2048], P('kv', 'tp'), may hold values from -0.09375 to 0.09375
- w_out: bfloat16 [2048, 4096], P('tp', 'kv'), may hold values from -0.125 to 0.125
- gain: float32 [4096], replicated, may hold values from 0.1 to 1.9
- head_gain: float32 [2048], replicated, may hold values from 0.1 to 1.9
- lower_bound: float32 [2048], replicated, may hold values from 0.05 to 0.9
- state: float32 [1024, 16, 128, 128], P(('grp', 'dp', 'kv'), 'tp'), parts along dimension 0, may hold values from -2.4 to 2.4
- last_forget: float32 [1024, 4, 2048], P(('grp', 'dp', 'kv'), None, 'tp'), parts along dimension 0, may hold values from 0.3 to 0.99
- last_values: bfloat16 [1024, 4, 2048], P(('grp', 'dp', 'kv'), None, 'tp'), parts along dimension 0, may hold values from -6 to 6
- accepted: int32 [1024], P(('grp', 'dp', 'kv')), parts along dimension 0, may hold values from 0 to 4
Outputs:
- mixed_out: bfloat16 [1024, 4, 4096], P(('grp', 'dp'), None, ('kv', 'tp')), parts along dimension 0
- taken: float32 [1024, 16, 128, 128], P(('grp', 'dp', 'kv'), 'tp'), parts along dimension 0
There are 2 independent parts, one for each index of `grp`. A program takes and returns all parts, laid end to end along the dimension named above; an argument that names none is the same for every part. Nothing has to cross between parts.
All inputs are finite; a program needn't handle non-finite values.
Results may differ from a plain program's by a relative error of at most 0.0071.
Values may be sent and summed in bfloat16 or wider, within the bound.
A program may use at most 64 MiB of HBM per device.

v0:
```python
import jax
import jax.numpy as jnp
from jax import lax
from jax.sharding import PartitionSpec as P

HEAD = 128


EPSILON = 1e-05
EXACT = lax.Precision.HIGHEST


def from_everyone(value, axis):
    copies = jnp.broadcast_to(value, (lax.axis_size(axis), *value.shape))
    return lax.all_to_all(copies, axis, split_axis=0, concat_axis=0, tiled=True)


def taken_together(value, axis):
    return from_everyone(value, axis).sum(axis=0)


def laid_out(pieces, dim):
    dims = list(pieces.shape[1:])
    dims[dim] *= pieces.shape[0]
    return jnp.moveaxis(pieces, 0, dim).reshape(dims)


def collect(value, axis, dim):
    return laid_out(from_everyone(value, axis), dim)


def cut_along(value, dim, peers):
    dims = value.shape
    pieces = value.reshape(*dims[:dim], peers, dims[dim] // peers, *dims[dim + 1 :])
    return jnp.moveaxis(pieces, dim, 0)


def sent_and_summed(value, axis, dim):
    pieces = cut_along(value, dim, lax.axis_size(axis))
    arrived = lax.all_to_all(pieces, axis, split_axis=0, concat_axis=0, tiled=True)
    return arrived.astype(jnp.float32).sum(axis=0)


def per_device(
    tokens,
    w_query,
    w_forget,
    w_input,
    w_gate,
    w_out,
    gain,
    head_gain,
    lower_bound,
    state,
    last_forget,
    last_values,
    accepted,
):
    group_seqs, props, feat_local = tokens.shape
    kv_count = lax.axis_size("kv")
    own_seqs = group_seqs // kv_count
    all_rows = group_seqs * props
    own_rows = own_seqs * props
    width = gain.shape[0]
    head_cols = w_query.shape[1]
    heads_dev = head_cols // HEAD
    kv_place = lax.axis_index("kv")
    tp_place = lax.axis_index("tp")
    flat_tokens = tokens.reshape(all_rows, feat_local)
    tokens_f32 = flat_tokens.astype(jnp.float32)
    gain_local = lax.dynamic_slice_in_dim(gain, kv_place * feat_local, feat_local)
    squares = taken_together(jnp.sum(tokens_f32 * tokens_f32, axis=1), "kv")
    row_scale = lax.rsqrt(squares / width + EPSILON)
    scaled = (tokens_f32 * gain_local).astype(jnp.bfloat16)
    stacked = jnp.concatenate([w_query, w_forget, w_input, w_gate], axis=1)
    block_rows = scaled
    product = jnp.dot(block_rows, stacked, preferred_element_type=jnp.float32)
    projected = lax.psum_scatter(product, "kv", scatter_dimension=0, tiled=True)
    projected = (
        projected * lax.dynamic_slice_in_dim(row_scale, kv_place * own_rows, own_rows, 0)[:, None]
    )
    projected = projected.reshape(own_rows, 4, head_cols)

    def shaped(array):
        return array.reshape(own_seqs, props, heads_dev, HEAD)

    floor_gate = lax.dynamic_slice_in_dim(lower_bound, tp_place * head_cols, head_cols).reshape(
        heads_dev, HEAD
    )
    gain_heads = lax.dynamic_slice_in_dim(head_gain, tp_place * head_cols, head_cols).reshape(
        heads_dev, HEAD
    )
    forget = floor_gate + (1.0 - floor_gate) * jax.nn.sigmoid(shaped(projected[:, 1]))
    keys_new = 1.0 - forget
    queries = jax.nn.silu(shaped(projected[:, 0])) * HEAD ** (-0.5)
    values_new = shaped(projected[:, 2])
    gate_path = jax.nn.silu(shaped(projected[:, 3]))
    old_forget = shaped(last_forget)
    old_values = shaped(last_values.astype(jnp.float32))
    accept_mask = (
        lax.broadcasted_iota(jnp.int32, (own_seqs, props), 1) < accepted[:, None]
    ).astype(jnp.float32)[:, :, None, None]
    old_cum = jnp.cumsum(accept_mask * jnp.log(old_forget), axis=1)
    old_end = old_cum[:, -1]
    old_weight = accept_mask * (1.0 - old_forget) * jnp.exp(old_end[:, None] - old_cum)
    taken = jnp.exp(old_end)[..., None] * state + jnp.einsum(
        "sphk,sphv->shkv", old_weight, old_values, precision=EXACT
    )
    new_cum = jnp.cumsum(jnp.log(forget), axis=1)
    carried = jnp.einsum("sthk,shkv->sthv", queries * jnp.exp(new_cum), taken, precision=EXACT)
    differences = new_cum[:, :, None] - new_cum[:, None, :]
    lower_pairs = (
        lax.broadcasted_iota(jnp.int32, (props, props), 0)
        >= lax.broadcasted_iota(jnp.int32, (props, props), 1)
    )[None, :, :, None, None]
    decay_pair = jnp.exp(jnp.where(lower_pairs, differences, -jnp.inf))
    scores = jnp.einsum("sthk,stuhk,suhk->shtu", queries, decay_pair, keys_new, precision=EXACT)
    recurrent = carried + jnp.einsum("shtu,suhv->sthv", scores, values_new, precision=EXACT)
    normed = recurrent * lax.rsqrt(jnp.mean(recurrent * recurrent, -1, keepdims=True) + EPSILON)
    heads_out = (
        (normed * gain_heads * gate_path).astype(jnp.bfloat16).reshape(own_seqs, props, head_cols)
    )
    block_rows = collect(heads_out, "kv", 0)
    part = jnp.dot(block_rows.reshape(-1, head_cols), w_out, preferred_element_type=jnp.float32)
    rounded = lax.optimization_barrier(part.astype(jnp.bfloat16)).astype(jnp.float32)
    terms = rounded.reshape(block_rows.shape[0], props, -1)
    mixed_out = sent_and_summed(terms.astype(jnp.bfloat16), "tp", 2).astype(jnp.bfloat16)
    return (mixed_out, taken)


def solution(mesh):
    in_specs = (
        P(("grp", "dp"), None, "kv"),
        P("kv", "tp"),
        P("kv", "tp"),
        P("kv", "tp"),
        P("kv", "tp"),
        P("tp", "kv"),
        P(),
        P(),
        P(),
        P(("grp", "dp", "kv"), "tp", None, None),
        P(("grp", "dp", "kv"), None, "tp"),
        P(("grp", "dp", "kv"), None, "tp"),
        P(("grp", "dp", "kv")),
    )
    out_specs = (P(("grp", "dp"), None, ("kv", "tp")), P(("grp", "dp", "kv"), "tp", None, None))
    return jax.shard_map(
        per_device, mesh=mesh, in_specs=in_specs, out_specs=out_specs, check_vma=False
    )
```

profile of v0, /device:TPU:65, one launch (start us, length us, event | category | flops | bytes accessed | tf_op | source)
XLA Modules:
  0.0 177.8 jit_solution(3959501910715042775)
XLA Ops:
  7.2 0.0 copy-start
  7.2 0.1 reduce-scatter.2.cloned.1.call-start
  7.3 1.0 reshape.93
  8.2 0.8 dynamic_slice.12
  9.0 4.2 %fusion = f32[256,4096]{1,0:T(8,128)} fusion(bf16[256,1024]{1,0:T(8,128)(2,1)} %param.17, bf16[256,1024]{1,0:T(8,128)(2,1)} %param.16, bf16[256,1024]{1,0:T(8,128)(2,1)} %param.15, bf16[256,1024]{1,0:T(8,128)(2,1)} %param.14, f32[256,256]{1,0:T(8,128)S(1)} %reshape.93, f32[256]{0:T(256)S(1)} %dynamic_slice.12), kind=kOutput, calls=%fused_computation | convolution fusion | flops 545390592 | bytes 6554624 | tf_op jit(solution)/shard_map/dot_general | solution.py:77
  13.2 0.0 copy-start.2
  13.2 0.0 copy-start.7
  13.2 0.0 copy-start.3
  13.2 0.0 copy-start.6
  13.2 0.0 copy-start.5
  13.2 0.0 copy-start.4
  13.2 0.1 reduce-scatter.2.cloned.1.call-update
  13.3 0.8 copy-done.2
  14.1 0.1 multiply_reduce_fusion
  14.2 0.1 broadcast_in_dim.18
  14.3 0.6 broadcast_in_dim.19
  14.9 44.2 %all-to-all-start = ((f32[16,1,256]{2,1,0:T(1,128)}), f32[16,1,256]{2,1,0:T(1,128)S(1)}, u32[]{:S(2)}, u32[]{:S(2)}) async-start(f32[16,1,256]{2,1,0:T(1,128)} %broadcast_in_dim.19), calls=%async_computation.1 | async-start | bytes 32768 | tf_op jit(solution)/shard_map/all_to_all | solution.py:15
  59.2 0.0 copy-done.7
  59.2 0.1 fusion.36
  59.3 0.0 copy-done.3
  59.3 0.1 bitcast_multiply_fusion.1
  59.3 0.1 reduce_window_sum.17
  59.5 0.0 copy-done.6
  59.5 0.0 copy-done.5
  59.6 0.0 copy-done.4
  59.6 3.8 %multiply_add_fusion = f32[4,8,128,128]{3,2,1,0:T(8,128)S(1)} fusion(f32[4,8,128,128]{3,2,1,0:T(8,128)} %param.22, f32[4,8,128]{2,1,0:T(8,128)S(1)} %exp.27, f32[4,4,8,128]{3,1,2,0:T(4,128)S(1)} %reduce_window_sum.17, f32[4,4,1024]{2,1,0:T(4,128)S(1)} %copy-done.3, bf16[4,4,1024]{2,1,0:T(4,128)(2,1)S(1)} %copy-done.4, f32[4,8,128]{2,1,0:T(8,128)S(1)} %bitcast.51, ...), kind=kOutput, calls=%fused_computation.8 | convolution fusion | flops 26279936 | bytes 4390976 | tf_op jit(solution)/shard_map/sphk,sphv->shkv/dot_general | solution.py:106
  63.3 0.0 copy-start.1
  63.4 7.0 %all-to-all-done = f32[16,1,256]{2,1,0:T(1,128)S(1)} async-done(((f32[16,1,256]{2,1,0:T(1,128)}), f32[16,1,256]{2,1,0:T(1,128)S(1)}, u32[]{:S(2)}, u32[]{:S(2)}) %all-to-all-start) | async-done | bytes 16416 | tf_op jit(solution)/shard_map/all_to_all | solution.py:15
  70.4 0.1 dynamic_slice.13
  70.5 50.6 %reduce-scatter.2.cloned.1.call-done = f32[16,4096]{1,0:T(8,128)} async-done(((f32[256,4096]{1,0:T(8,128)}), f32[16,4096]{1,0:T(8,128)}) %reduce-scatter.2.cloned.1.call-update) | async-done | bytes 262160 | tf_op jit(solution)/shard_map/reduce_scatter | solution.py:78
  121.1 1.0 broadcast_multiply_fusion
  122.1 0.2 reshape.91
  122.3 0.2 fusion.40
  122.6 0.1 reduce_window_sum.18
  122.8 1.9 %fusion.21 = f32[4,8,128,4]{2,3,1,0:T(4,128)S(1)} fusion(f32[4,8,128,128]{3,2,1,0:T(8,128)S(1)} %multiply_add_fusion, f32[4,4,8,128]{3,1,2,0:T(4,128)S(1)} %reduce_window_sum.18, f32[4,4,8,128]{3,2,1,0:T(8,128)S(1)} %bitcast.45), kind=kOutput, calls=%fused_computation.35 | convolution fusion | flops 25264128 | bytes 2293760 | tf_op jit(solution)/shard_map/sthk,shkv->sthv/dot_general | solution.py:110
  124.7 0.0 copy-done.1
  124.7 0.1 multiply_bitcast_fusion
  124.9 1.0 fusion.9
  125.8 0.4 multiply_reduce_fusion.1
  126.3 0.1 fusion.35
  126.4 0.2 broadcast_in_dim.34
  126.6 24.6 %all_to_all.16 = bf16[16,4,4,1024]{3,2,1,0:T(4,128)(2,1)S(1)} all-to-all(bf16[16,4,4,1024]{3,2,1,0:T(4,128)(2,1)S(1)} %broadcast_in_dim.34), channel_id=1, replica_groups=mesh['grp'=2,'dp'=8,'kv'=16,'tp'=2] {'kv'}, dimensions={0} | all-to-all | bytes 1048576 | tf_op jit(solution)/shard_map/all_to_all | solution.py:15
  151.2 0.1 reshape_reshape.3
  151.3 0.0 copy-done
  151.3 0.3 convolution_convert_fusion
  151.7 18.5 %all_to_all.17 = bf16[2,64,4,128]{3,2,1,0:T(4,128)(2,1)S(1)} all-to-all(bf16[2,64,4,128]{3,2,1,0:T(4,128)(2,1)S(1)} %bitcast.46), channel_id=1, replica_groups=mesh['grp'=2,'dp'=8,'kv'=16,'tp'=2] {'tp'}, dimensions={0} | all-to-all | bytes 262144 | tf_op jit(solution)/shard_map/all_to_all | solution.py:40
  170.2 0.7 reduce_sum.42
  (16 shorter events, 0.3 us)
Async XLA Ops:
  7.2 144.1 %copy-start = (bf16[1024,256]{1,0:T(8,128)(2,1)S(1)}, bf16[1024,256]{1,0:T(8,128)(2,1)}, u32[]{:S(2)}) copy-start(bf16[1024,256]{1,0:T(8,128)(2,1)} %param.18) | copy-start | bytes 1572868
  7.2 113.9 %reduce-scatter.2.cloned.1.call-start = ((), (), s32[]{:S(2)}) async-start(), calls=%async_computation.4 | async-start | bytes 4456448 | tf_op jit(solution)/shard_map/reduce_scatter | solution.py:78
  13.2 0.9 copy-start.2
  13.2 46.0 %copy-start.7 = (s32[4]{0:T(128)S(1)}, s32[4]{0:T(128)}, u32[]{:S(2)}) copy-start(s32[4]{0:T(128)} %param.25) | copy-start | bytes 52
  13.2 46.1 %copy-start.3 = (f32[4,4,1024]{2,1,0:T(4,128)S(1)}, f32[4,4,1024]{2,1,0:T(4,128)}, u32[]{:S(2)}) copy-start(f32[4,4,1024]{2,1,0:T(4,128)} %param.23) | copy-start | bytes 196612
  13.2 46.3 %copy-start.6 = (f32[2048]{0:T(1024)S(1)}, f32[2048]{0:T(1024)}, u32[]{:S(2)}) copy-start(f32[2048]{0:T(1024)} %param.20) | copy-start | bytes 24580
  13.2 46.4 %copy-start.5 = (f32[2048]{0:T(1024)S(1)}, f32[2048]{0:T(1024)}, u32[]{:S(2)}) copy-start(f32[2048]{0:T(1024)} %param.21) | copy-start | bytes 24580
  13.2 46.4 %copy-start.4 = (bf16[4,4,1024]{2,1,0:T(4,128)(2,1)S(1)}, bf16[4,4,1024]{2,1,0:T(4,128)(2,1)}, u32[]{:S(2)}) copy-start(bf16[4,4,1024]{2,1,0:T(4,128)(2,1)} %param.24) | copy-start | bytes 98308
  14.9 55.4 %all-to-all-start = ((f32[16,1,256]{2,1,0:T(1,128)}), f32[16,1,256]{2,1,0:T(1,128)S(1)}, u32[]{:S(2)}, u32[]{:S(2)}) async-start(f32[16,1,256]{2,1,0:T(1,128)} %broadcast_in_dim.19), calls=%async_computation.1 | async-start | bytes 32768 | tf_op jit(solution)/shard_map/all_to_all | solution.py:15
  63.3 61.4 %copy-start.1 = (f32[4,8,128,128]{3,2,1,0:T(8,128)}, f32[4,8,128,128]{3,2,1,0:T(8,128)S(1)}, u32[]{:S(2)}) copy-start(f32[4,8,128,128]{3,2,1,0:T(8,128)S(1)} %multiply_add_fusion) | copy-start | bytes 6291460
Sparse Core Ops, SparseCore 0:
  13.4 107.6 reduce-scatter.1
where the time goes:
time: 178 us
  waiting for transfers between devices  57.7 us (32%)
  starting transfers between devices  44.3 us (25%)
  blocking collectives  43.1 us (24%)
  between operations  14.3 us (8%)
  matrix products  11.5 us (6%)
  local copies, waits for them, and re-layouts  4.2 us (2%)
  other arithmetic  2.67 us (2%)
    reduce_scatter x1, waiting for transfers between devices, per_device(): projected = lax.psum_scatter(product, 'kv', scatter_dimension=0, tiled=True)  50.6 us
    all_to_all x1, starting transfers between devices, from_everyone(): return lax.all_to_all(copies, axis, split_axis=0, concat_axis=0, tiled=True)  44.2 us
    all_to_all x1, blocking collectives, from_everyone(): return lax.all_to_all(copies, axis, split_axis=0, concat_axis=0, tiled=True)  24.6 us
    all_to_all x1, blocking collectives, sent_and_summed(): lax.all_to_all(pieces, axis, split_axis=0, concat_axis=0, tiled=True)  18.5 us
    all_to_all x1, waiting for transfers between devices, from_everyone(): return lax.all_to_all(copies, axis, split_axis=0, concat_axis=0, tiled=True)  7 us
    dot_general x1, matrix products, per_device(): product = jnp.dot(block_rows, stacked, preferred_element_type=jnp.float32)  4.16 us
    dot_general x1, matrix products, per_device(): jnp.einsum('sphk,sphv->shkv', old_weight, old_values, precision=EXACT)  3.76 us
  transfers between devices with their start and end apart: 2, of which 2 were waited for; matrix products, arithmetic and copies ran while one was open for 3% of the time, Pallas kernels for 0%

commit v1 on v0

v1 whole, which is shorter than its diff:
```python
import functools

import jax
import jax.numpy as jnp
from jax import lax
from jax.experimental import pallas as pl
from jax.experimental.pallas import tpu as pltpu
from jax.sharding import PartitionSpec as P

HEAD = 128
EPSILON = 1e-05
PIECES = 4
RIGHT, LEFT = 0, 1
F32, BF16 = jnp.float32, jnp.bfloat16


def split(value):
    high = value.astype(BF16)
    return high, (value - high.astype(F32)).astype(BF16)


def kernel(
    n,
    tokens,
    w_query,
    w_forget,
    w_input,
    w_gate,
    w_out,
    gain,
    head_gain,
    lower_bound,
    state,
    last_forget,
    last_values,
    accepted,
    mixed,
    taken,
    tok_v,
    w_v,
    wo_v,
    state_v,
    taken_v,
    t_high,
    t_low,
    columns,
    product,
    squares,
    sums_out,
    sums_in,
    sq_out,
    sq_in,
    gathered,
    halves,
    other,
    load_sem,
    w_sem,
    state_sem,
    taken_sem,
    sum_send,
    sum_recv,
    sq_send,
    sq_recv,
    all_send,
    all_recv,
    half_send,
    half_recv,
):
    half_n = n // 2
    me = lax.axis_index("kv")
    core = lax.axis_index("tp")
    seqs, props, feat = tokens.shape
    rows = seqs * props
    own = rows // n
    own_seqs = own // props
    cols = w_query.shape[1]
    heads = cols // HEAD
    wide = cols // PIECES
    per_piece = wide // HEAD
    width = gain.shape[0] * gain.shape[1]
    weights = (w_query, w_forget, w_input, w_gate)

    def at(offset):
        return lax.rem(me + offset + 2 * n, n)

    load_tok = pltpu.make_async_copy(tokens, tok_v, load_sem.at[0])
    load_tok.start()
    w_loads = []
    for p in range(PIECES):
        for x in range(4):
            part = pl.ds(p * wide, wide)
            copy = pltpu.make_async_copy(
                weights[x].at[:, part], w_v.at[x, :, part], w_sem.at[p, x]
            )
            copy.start()
            w_loads.append(copy)
    s_loads = []
    for h in range(heads):
        copy = pltpu.make_async_copy(state.at[:, h], state_v.at[:, h], state_sem.at[h])
        copy.start()
        s_loads.append(copy)
    load_wo = pltpu.make_async_copy(w_out, wo_v, load_sem.at[1])
    load_wo.start()

    barrier = pltpu.get_barrier_semaphore()
    for peer in ({"kv": at(1)}, {"kv": at(-1)}, {"tp": 1 - core}):
        pl.semaphore_signal(
            barrier, inc=1, device_id=peer, device_id_type=pl.DeviceIdType.MESH
        )

    def remote(src, dst, send_sem, recv_sem, peer):
        return pltpu.make_async_remote_copy(
            src_ref=src,
            dst_ref=dst,
            send_sem=send_sem,
            recv_sem=recv_sem,
            device_id=peer,
            device_id_type=pl.DeviceIdType.MESH,
        )

    def sum_copy(way, step, p):
        return remote(
            sums_out.at[way, step - 1, p],
            sums_in.at[way, step - 1, p],
            sum_send.at[way, step - 1, p],
            sum_recv.at[way, step - 1, p],
            {"kv": at(1 if way == RIGHT else -1)},
        )

    def sq_copy(way, step):
        return remote(
            sq_out.at[way, step - 1],
            sq_in.at[way, step - 1],
            sq_send.at[way, step - 1],
            sq_recv.at[way, step - 1],
            {"kv": at(1 if way == RIGHT else -1)},
        )

    def first_way(p):
        return RIGHT if p < PIECES // 2 else LEFT

    load_tok.wait()
    tok = tok_v[...].astype(F32).reshape(rows, feat)
    gain_row = jnp.concatenate(
        [gain[pl.ds(me * (feat // 128) + i, 1), :] for i in range(feat // 128)], axis=1
    )
    scaled = (tok * gain_row).astype(BF16)

    pl.semaphore_wait(barrier, 3)

    def products(p):
        for x in range(4):
            w_loads[p * 4 + x].wait()
            out = jnp.dot(
                scaled, w_v[x, :, p * wide : (p + 1) * wide], preferred_element_type=F32
            )
            product[p, :, :, x * wide : (x + 1) * wide] = out.reshape(n, own, wide)

    def start_sum(way, step, p):
        dist = half_n + 1 - step
        value = product[p, at(dist if way == RIGHT else -dist)]
        fresh = step == 1 or (step == 2 and first_way(p) != way)
        if not fresh:
            sum_copy(way, step - 1, p).wait_recv()
            value = value + sums_in[way, step - 2, p].astype(F32)
        sums_out[way, step - 1, p] = value.astype(BF16)
        sum_copy(way, step, p).start()

    def start_sq(way, step):
        dist = half_n + 1 - step
        value = squares[at(dist if way == RIGHT else -dist)]
        fresh = step == 1 or (step == 2 and way == LEFT)
        if not fresh:
            sq_copy(way, step - 1).wait_recv()
            value = value + sq_in[way, step - 2]
        sq_out[way, step - 1] = value
        sq_copy(way, step).start()

    for p in range(PIECES):
        products(p)
        start_sum(first_way(p), 1, p)

    row_sum = jnp.sum(tok * tok, axis=1, keepdims=True)
    spread = jnp.where(
        lax.rem(lax.broadcasted_iota(jnp.int32, (rows, 128), 0), own)
        == lax.broadcasted_iota(jnp.int32, (rows, 128), 1),
        row_sum,
        0.0,
    )
    squares[...] = jnp.sum(spread.reshape(n, own, 128), axis=1, keepdims=True)
    start_sq(RIGHT, 1)

    row_of = lax.broadcasted_iota(jnp.int32, (own, 1), 0)
    pos = lax.rem(row_of, props)
    seq_of = row_of // props
    limit = jnp.zeros((own, 1), jnp.int32)
    for s in range(own_seqs):
        limit = jnp.where(seq_of == s, accepted[s], limit)

    def prepare():
        old = last_forget[...].reshape(own, cols)
        kept = pos < limit
        factor = jnp.where(kept, old, 1.0)
        after = jnp.ones_like(factor)
        for step in range(1, props):
            shifted = pltpu.roll(factor, own - step, 0)
            after = after * jnp.where(pos < props - step, shifted, 1.0)
        weight = jnp.where(kept, 1.0 - old, 0.0) * after
        decay = factor * after
        pack = 128 // (2 * own)
        for group in range(heads // pack):
            stack = []
            for h in range(group * pack, (group + 1) * pack):
                stack.append(weight[:, h * HEAD : (h + 1) * HEAD])
                stack.append(decay[:, h * HEAD : (h + 1) * HEAD])
            columns[group] = jnp.concatenate(stack, axis=0).T

    def take(h):
        s_loads[h].wait()
        pack = 128 // (2 * own)
        base = (h % pack) * 2 * own
        table = columns[h // pack]
        values = last_values[:, :, h * HEAD : (h + 1) * HEAD].astype(F32)
        for s in range(own_seqs):
            at_decay = base + own + s * props
            total = table[:, at_decay : at_decay + 1] * state_v[s, h]
            for j in range(props):
                at_weight = base + s * props + j
                total = total + table[:, at_weight : at_weight + 1] * values[s, j : j + 1]
            taken_v[s, h] = total
            high, low = split(total)
            t_high[h, s * HEAD : (s + 1) * HEAD, :] = high
            t_low[h, s * HEAD : (s + 1) * HEAD, :] = low
        pltpu.make_async_copy(taken_v.at[:, h], taken.at[:, h], taken_sem.at[h]).start()

    done = 0
    for step in range(2, half_n + 1):
        if step == 2:
            for p in range(PIECES):
                start_sum(1 - first_way(p), 2, p)
            start_sq(LEFT, 2)
            prepare()
            for p in range(PIECES):
                start_sum(first_way(p), 2, p)
            start_sq(RIGHT, 2)
        else:
            for p in range(PIECES):
                start_sum(RIGHT, step, p)
                start_sum(LEFT, step, p)
            start_sq(RIGHT, step)
            start_sq(LEFT, step)
        until = heads * (step - 1) // (half_n - 1)
        for h in range(done, until):
            take(h)
        done = until

    sq_copy(RIGHT, half_n).wait_recv()
    sq_copy(LEFT, half_n).wait_recv()
    square = squares[me] + sq_in[RIGHT, half_n - 1] + sq_in[LEFT, half_n - 1]
    square = jnp.sum(
        jnp.where(
            lax.broadcasted_iota(jnp.int32, (own, 128), 0)
            == lax.broadcasted_iota(jnp.int32, (own, 128), 1),
            square,
            0.0,
        ),
        axis=1,
        keepdims=True,
    )
    row_scale = lax.rsqrt(square / width + EPSILON)

    def all_copy(src_slot, dst_slot, p, offset):
        return remote(
            gathered.at[src_slot, p],
            gathered.at[dst_slot, p],
            all_send.at[dst_slot, p],
            all_recv.at[dst_slot, p],
            {"kv": at(offset)},
        )

    def spread_from(slot, p):
        if slot < half_n:
            for offset in (1, 2):
                if slot + offset <= half_n:
                    all_copy(slot, slot + offset, p, offset).start()
        if slot == 0 or slot > half_n:
            back = (n - slot) % n
            for offset in (1, 2):
                if back + offset < half_n:
                    all_copy(slot, n - back - offset, p, -offset).start()

    def head_out(p, j, fin):
        h = p * per_piece + j
        lanes = [slice(x * wide + j * HEAD, x * wide + (j + 1) * HEAD) for x in range(4)]
        floor_gate = lower_bound[pl.ds(core * heads + h, 1), :]
        gain_head = head_gain[pl.ds(core * heads + h, 1), :]
        query = jax.nn.silu(fin[:, lanes[0]]) * HEAD ** (-0.5)
        forget = floor_gate + (1.0 - floor_gate) * jax.nn.sigmoid(fin[:, lanes[1]])
        key = 1.0 - forget
        value = fin[:, lanes[2]]
        gate = jax.nn.silu(fin[:, lanes[3]])
        recurrent = jnp.sum(query * key, axis=1, keepdims=True) * value
        decay = query
        for lag in range(1, props):
            ok = pos >= lag
            decay = decay * jnp.where(pos >= lag - 1, pltpu.roll(forget, lag - 1, 0), 1.0)
            score = jnp.sum(decay * pltpu.roll(key, lag, 0), axis=1, keepdims=True)
            recurrent = recurrent + jnp.where(ok, score, 0.0) * pltpu.roll(value, lag, 0)
        decay = decay * jnp.where(pos >= props - 1, pltpu.roll(forget, props - 1, 0), 1.0)
        left = jnp.concatenate(
            [jnp.where(seq_of == s, decay, 0.0) for s in range(own_seqs)], axis=1
        )
        high, low = split(left)
        carried = jnp.dot(
            jnp.concatenate([high, low], axis=0), t_high[h], preferred_element_type=F32
        )
        recurrent = (
            recurrent
            + carried[:own]
            + carried[own:]
            + jnp.dot(high, t_low[h], preferred_element_type=F32)
        )
        mean = jnp.mean(recurrent * recurrent, axis=1, keepdims=True)
        return (recurrent * lax.rsqrt(mean + EPSILON) * gain_head * gate).astype(BF16)

    for p in range(PIECES):
        sum_copy(RIGHT, half_n, p).wait_recv()
        sum_copy(LEFT, half_n, p).wait_recv()
        fin = (
            product[p, me]
            + sums_in[RIGHT, half_n - 1, p].astype(F32)
            + sums_in[LEFT, half_n - 1, p].astype(F32)
        ) * row_scale
        for j in range(per_piece):
            gathered[0, p, :, j * HEAD : (j + 1) * HEAD] = head_out(p, j, fin)
        spread_from(0, p)

    relays = []
    for near in range(2, half_n, 2):
        relays += [near, n - near]
    for slot in relays:
        for p in range(PIECES):
            all_copy(0, slot, p, 1).wait_recv()
            spread_from(slot, p)
    for slot in range(1, n):
        if slot not in relays:
            for p in range(PIECES):
                all_copy(0, slot, p, 1).wait_recv()

    load_wo.wait()
    total = jnp.zeros((rows, wo_v.shape[1]), F32)
    for p in range(PIECES):
        total = total + jnp.dot(
            gathered[:, p].reshape(rows, wide),
            wo_v[p * wide : (p + 1) * wide, :],
            preferred_element_type=F32,
        )
    out_cols = wo_v.shape[1] // 2
    for c in range(2):
        halves[c] = total[:, c * out_cols : (c + 1) * out_cols].astype(BF16)
    swap = remote(
        halves.at[1 - core], other, half_send.at[0], half_recv.at[0], {"tp": 1 - core}
    )
    swap.start()
    swap.wait_recv()
    result = (halves[core].astype(F32) + other[...].astype(F32)).astype(BF16)
    result = result.reshape(n, own_seqs, props, out_cols)
    for slot in range(n):
        mixed[pl.ds(at(-slot) * own_seqs, own_seqs)] = result[slot]

    swap.wait_send()
    for h in range(heads):
        pltpu.make_async_copy(taken_v.at[:, h], taken.at[:, h], taken_sem.at[h]).wait()
    for p in range(PIECES):
        for way in (RIGHT, LEFT):
            for step in range(1, half_n + 1):
                if step > 1 or first_way(p) == way:
                    sum_copy(way, step, p).wait_send()
        for slot in range(1, n):
            all_copy(0, slot, p, 1).wait_send()
    for way in (RIGHT, LEFT):
        for step in range(1, half_n + 1):
            if step > 1 or way == RIGHT:
                sq_copy(way, step).wait_send()


def per_device(
    tokens,
    w_query,
    w_forget,
    w_input,
    w_gate,
    w_out,
    gain,
    head_gain,
    lower_bound,
    state,
    last_forget,
    last_values,
    accepted,
):
    n = lax.axis_size("kv")
    half_n = n // 2
    seqs, props, feat = tokens.shape
    rows = seqs * props
    own = rows // n
    cols = w_query.shape[1]
    heads = cols // HEAD
    wide = cols // PIECES
    out_cols = w_out.shape[1]
    any_space = pl.BlockSpec(memory_space=pl.ANY)
    vmem = pl.BlockSpec(memory_space=pltpu.VMEM)
    dma = pltpu.SemaphoreType.DMA
    return pl.pallas_call(
        functools.partial(kernel, n),
        out_shape=(
            jax.ShapeDtypeStruct((seqs, props, out_cols // 2), BF16),
            jax.ShapeDtypeStruct(state.shape, F32),
        ),
        in_specs=[any_space] * 6
        + [vmem] * 3
        + [any_space]
        + [vmem] * 2
        + [pl.BlockSpec(memory_space=pltpu.SMEM)],
        out_specs=(vmem, any_space),
        scratch_shapes=[
            pltpu.VMEM((seqs, props, feat), BF16),
            pltpu.VMEM((4, feat, cols), BF16),
            pltpu.VMEM(w_out.shape, BF16),
            pltpu.VMEM(state.shape, F32),
            pltpu.VMEM(state.shape, F32),
            pltpu.VMEM((heads, own // props * HEAD, HEAD), BF16),
            pltpu.VMEM((heads, own // props * HEAD, HEAD), BF16),
            pltpu.VMEM((heads * 2 * own // 128, 128, 128), F32),
            pltpu.VMEM((PIECES, n, own, 4 * wide), F32),
            pltpu.VMEM((n, 1, 128), F32),
            pltpu.VMEM((2, half_n, PIECES, own, 4 * wide), BF16),
            pltpu.VMEM((2, half_n, PIECES, own, 4 * wide), BF16),
            pltpu.VMEM((2, half_n, 1, 128), F32),
            pltpu.VMEM((2, half_n, 1, 128), F32),
            pltpu.VMEM((n, PIECES, own, wide), BF16),
            pltpu.VMEM((2, rows, out_cols // 2), BF16),
            pltpu.VMEM((rows, out_cols // 2), BF16),
            dma((2,)),
            dma((PIECES, 4)),
            dma((heads,)),
            dma((heads,)),
            dma((2, half_n, PIECES)),
            dma((2, half_n, PIECES)),
            dma((2, half_n)),
            dma((2, half_n)),
            dma((n, PIECES)),
            dma((n, PIECES)),
            dma((1,)),
            dma((1,)),
        ],
        compiler_params=pltpu.CompilerParams(
            collective_id=0, has_side_effects=True, vmem_limit_bytes=67043328
        ),
    )(
        tokens,
        w_query,
        w_forget,
        w_input,
        w_gate,
        w_out,
        gain.reshape(-1, 128),
        head_gain.reshape(-1, 128),
        lower_bound.reshape(-1, 128),
        state,
        last_forget,
        last_values,
        accepted,
    )


def solution(mesh):
    in_specs = (
        P(("grp", "dp"), None, "kv"),
        P("kv", "tp"),
        P("kv", "tp"),
        P("kv", "tp"),
        P("kv", "tp"),
        P("tp", "kv"),
        P(),
        P(),
        P(),
        P(("grp", "dp", "kv"), "tp", None, None),
        P(("grp", "dp", "kv"), None, "tp"),
        P(("grp", "dp", "kv"), None, "tp"),
        P(("grp", "dp", "kv")),
    )
    out_specs = (P(("grp", "dp"), None, ("kv", "tp")), P(("grp", "dp", "kv"), "tp", None, None))
    return jax.shard_map(
        per_device, mesh=mesh, in_specs=in_specs, out_specs=out_specs, check_vma=False
    )
```

time: 178 us -> 102 us (0.57)
  Pallas kernels: 0 us -> 96.9 us
  waiting for transfers between devices: 57.7 us -> 0 us
  starting transfers between devices: 44.3 us -> 0 us
  blocking collectives: 43.1 us -> 0 us
  between operations: 14.3 us -> 0.64 us
  matrix products: 11.5 us -> 0 us
  other arithmetic: 2.67 us -> 0 us
    pallas_call x0 -> x1, Pallas kernels: none -> 96.9 us  [per_device(): pl.pallas_call(functools.partial(kernel, n), out_shape=(jax.ShapeDtypeStr...]
    reduce_scatter x1 -> x0, waiting for transfers between devices: 50.6 us -> none  [per_device(): projected = lax.psum_scatter(product, 'kv', scatter_dimension=0, tiled=True)]
    all_to_all x1 -> x0, starting transfers between devices: 44.2 us -> none  [from_everyone(): return lax.all_to_all(copies, axis, split_axis=0, concat_axis=0, tiled=True)]
    all_to_all x2 -> x0, blocking collectives: 43.1 us -> none  [the longest x1 24.6 us: from_everyone(): return lax.all_to_all(copies, axis, split_axis=0, concat_axis=0, tiled=True)]
    dot_general x6 -> x0, matrix products: 11.5 us -> none  [the longest x1 4.16 us: per_device(): product = jnp.dot(block_rows, stacked, preferred_element_type=jnp.float32)]
    all_to_all x1 -> x0, waiting for transfers between devices: 7 us -> none  [from_everyone(): return lax.all_to_all(copies, axis, split_axis=0, concat_axis=0, tiled=True)]
    unnamed x17 -> x2, local copies, waits for them, and re-layouts: 0.86 us -> 4.63 us
  transfers between devices with their start and end apart: 2 -> 0, of which waited for: 2 -> 0; matrix products, arithmetic and copies ran while one was open for 3% -> 0% of each run, Pallas kernels for 0% -> 0%
where the time goes in v1:
time: 102 us
  Pallas kernels  96.9 us (95%)
  local copies, waits for them, and re-layouts  4.63 us (5%)
    pallas_call x1, Pallas kernels, per_device(): pl.pallas_call(functools.partial(kernel, n), out_shape=(jax.ShapeDtypeStr...  96.9 us
    unnamed x2, local copies, waits for them, and re-layouts  4.63 us

profile of v1, /device:TPU:65, one launch (start us, length us, event | category | flops | bytes accessed | tf_op | source)
XLA Modules:
  0.0 102.2 jit_solution(12262085792164668354)
XLA Ops:
  0.6 96.9 %shard_map.140 = (bf16[64,4,128]{2,1,0:T(4,128)(2,1)}, f32[4,8,128,128]{3,2,1,0:T(8,128)}) custom-call(bf16[64,4,256]{2,1,0:T(4,128)(2,1)} %tokens.1, bf16[256,1024]{1,0:T(8,128)(2,1)} %w_query.1, bf16[256,1024]{1,0:T(8,128)(2,1)} %w_forget.1, bf16[256,1024]{1,0:T(8,128)(2,1)} %w_input.1, bf16[256,1024]{1,0:T(8,128)(2,1)} %w_gate.1, ...), custom_call_target="tpu_custom_call" | custom-call | tf_op jit(solution)/shard_map/pallas_call | solution.py:414
  97.6 1.5 %copy.17 = bf16[64,4,128]{2,1,0:T(4,128)(2,1)} copy(bf16[64,4,128]{2,1,0:T(4,128)(2,1)} %get-tuple-element.4) | data formatting | bytes 131072
  99.1 3.1 %copy.18 = f32[4,8,128,128]{3,2,1,0:T(8,128)} copy(f32[4,8,128,128]{3,2,1,0:T(8,128)} %get-tuple-element.5) | data formatting | bytes 4194304

commit v2 on v1

v2 whole, which is shorter than its diff:
```python
import functools

import jax
import jax.numpy as jnp
from jax import lax
from jax.experimental import pallas as pl
from jax.experimental.pallas import tpu as pltpu
from jax.sharding import PartitionSpec as P

HEAD = 128
EPSILON = 1e-05
GROUPS = 4
SUB = 2
PIECES = GROUPS * SUB
RIGHT, LEFT = 0, 1
F32, BF16 = jnp.float32, jnp.bfloat16


def column_order(n):
    passed = [n - s if back else s for s in range(2, n // 2, 2) for back in (0, 1)]
    return [0] + passed + [s for s in range(1, n) if s not in passed]


def split(value):
    high = value.astype(BF16)
    return high, (value - high.astype(F32)).astype(BF16)


def kernel(
    n,
    tokens,
    w_query,
    w_forget,
    w_input,
    w_gate,
    w_out,
    gain_h,
    head_gain_h,
    lower_bound_h,
    state,
    last_forget_h,
    last_values_h,
    accepted_h,
    mixed,
    taken,
    accepted,
    gain,
    head_gain,
    lower_bound,
    last_forget,
    last_values,
    tok_v,
    scaled_v,
    w_v,
    wo_v,
    state_v,
    t_high,
    t_low,
    weight_v,
    decay_v,
    columns,
    product,
    squares,
    sums_out,
    sums_in,
    sq_out,
    sq_in,
    gathered,
    halves,
    other,
    load_sem,
    w_sem,
    sum_send,
    sum_recv,
    sq_send,
    sq_recv,
    all_send,
    all_recv,
    half_send,
    half_recv,
):
    half_n = n // 2
    me = lax.axis_index("kv")
    core = lax.axis_index("tp")
    seqs, props, feat = tokens.shape
    rows = seqs * props
    own = rows // n
    own_seqs = own // props
    cols = w_query.shape[1]
    heads = cols // HEAD
    wide = cols // PIECES
    per_piece = wide // HEAD
    width = gain.shape[0] * gain.shape[1]
    weights = (w_query, w_forget, w_input, w_gate)

    def at(offset):
        return lax.rem(me + offset + 2 * n, n)

    barrier = pltpu.get_barrier_semaphore()
    for peer in ({"kv": at(1)}, {"kv": at(-1)}, {"tp": 1 - core}):
        pl.semaphore_signal(
            barrier, inc=1, device_id=peer, device_id_type=pl.DeviceIdType.MESH
        )

    load_tok = pltpu.make_async_copy(tokens, tok_v, load_sem.at[0])
    load_tok.start()
    small = []
    for i, (src, dst) in enumerate(
        (
            (gain_h, gain),
            (head_gain_h, head_gain),
            (lower_bound_h, lower_bound),
            (last_forget_h, last_forget),
            (last_values_h, last_values),
            (accepted_h, accepted),
        )
    ):
        small.append(pltpu.make_async_copy(src, dst, load_sem.at[2 + i]))
    small[0].start()
    w_loads = []
    for x in range(4):
        copy = pltpu.make_async_copy(weights[x], w_v.at[x], w_sem.at[x])
        copy.start()
        w_loads.append(copy)
    for copy in small[1:]:
        copy.start()
    load_state = pltpu.make_async_copy(state, state_v, load_sem.at[8])
    load_state.start()
    load_wo = pltpu.make_async_copy(w_out, wo_v, load_sem.at[1])
    load_wo.start()

    def remote(src, dst, send_sem, recv_sem, peer):
        return pltpu.make_async_remote_copy(
            src_ref=src,
            dst_ref=dst,
            send_sem=send_sem,
            recv_sem=recv_sem,
            device_id=peer,
            device_id_type=pl.DeviceIdType.MESH,
        )

    def slot_of(way, step, p, pieces):
        if step == 1:
            return 2 * (half_n - 1) * pieces + p
        return (way * (half_n - 1) + step - 2) * pieces + p

    def sum_copy(way, step, p):
        slot = slot_of(way, step, p, PIECES)
        return remote(
            sums_out.at[slot],
            sums_in.at[slot],
            sum_send.at[0],
            sum_recv.at[slot],
            {"kv": at(1 if way == RIGHT else -1)},
        )

    def sq_copy(way, step):
        slot = slot_of(way, step, 0, 1)
        return remote(
            sq_out.at[slot],
            sq_in.at[slot],
            sq_send.at[0],
            sq_recv.at[slot],
            {"kv": at(1 if way == RIGHT else -1)},
        )

    def first_way(p):
        return RIGHT if p % 2 == 0 else LEFT

    load_tok.wait()
    small[0].wait()
    tok = tok_v[...].astype(F32).reshape(rows, feat)
    gain_row = jnp.concatenate(
        [gain[pl.ds(me * (feat // 128) + i, 1), :] for i in range(feat // 128)], axis=1
    )
    scaled_v[...] = (tok * gain_row).astype(BF16)

    with jax.named_scope("k_barrier"):
        pl.semaphore_wait(barrier, 3)

    def products(g):
        out = jnp.dot(
            scaled_v[...],
            jnp.concatenate(
                [w_v[x, :, g * SUB * wide : (g + 1) * SUB * wide] for x in range(4)], axis=1
            ),
            preferred_element_type=F32,
        )
        for x in range(4):
            for j in range(SUB):
                column = (x * SUB + j) * wide
                product[g * SUB + j, :, :, x * wide : (x + 1) * wide] = out[
                    :, column : column + wide
                ].reshape(n, own, wide)

    for copy in w_loads:
        copy.wait()

    def start_sum(way, step, p):
        dist = half_n + 1 - step
        value = product[p, at(dist if way == RIGHT else -dist)]
        fresh = step == 1 or (step == 2 and first_way(p) != way)
        if not fresh:
            sum_copy(way, step - 1, p).wait_recv()
            value = value + sums_in[slot_of(way, step - 1, p, PIECES)].astype(F32)
        sums_out[slot_of(way, step, p, PIECES)] = value.astype(BF16)
        sum_copy(way, step, p).start()

    def start_sq(way, step):
        dist = half_n + 1 - step
        value = squares[at(dist if way == RIGHT else -dist)]
        fresh = step == 1 or (step == 2 and way == LEFT)
        if not fresh:
            sq_copy(way, step - 1).wait_recv()
            value = value + sq_in[slot_of(way, step - 1, 0, 1)]
        sq_out[slot_of(way, step, 0, 1)] = value
        sq_copy(way, step).start()

    for g in range(GROUPS):
        products(g)
        for p in range(g * SUB, (g + 1) * SUB):
            start_sum(first_way(p), 1, p)
            start_sum(1 - first_way(p), 2, p)

    row_sum = jnp.sum(tok * tok, axis=1, keepdims=True)
    spread = jnp.where(
        lax.rem(lax.broadcasted_iota(jnp.int32, (rows, 128), 0), own)
        == lax.broadcasted_iota(jnp.int32, (rows, 128), 1),
        row_sum,
        0.0,
    )
    squares[...] = jnp.sum(spread.reshape(n, own, 128), axis=1, keepdims=True)
    start_sq(RIGHT, 1)

    row_of = lax.broadcasted_iota(jnp.int32, (own, 1), 0)
    pos = lax.rem(row_of, props)
    seq_of = row_of // props
    def prepare():
        for copy in small[1:]:
            copy.wait()
        limit = jnp.zeros((own, 1), jnp.int32)
        for s in range(own_seqs):
            limit = jnp.where(seq_of == s, accepted[s], limit)
        old = last_forget[...].reshape(own, cols)
        kept = pos < limit
        factor = jnp.where(kept, old, 1.0)
        after = jnp.ones_like(factor)
        for step in range(1, props):
            shifted = pltpu.roll(factor, own - step, 0)
            after = after * jnp.where(pos < props - step, shifted, 1.0)
        weight = jnp.where(kept, 1.0 - old, 0.0) * after
        decay = factor * after
        for h in range(heads):
            lanes = slice(h * HEAD, (h + 1) * HEAD)
            weight_v[h] = weight[:, lanes]
            decay_v[h * own : (h + 1) * own, :] = decay[:, lanes]
        columns[...] = decay_v[...].T
        load_state.wait()

    def blocks(value):
        return jnp.concatenate(
            [jnp.where(seq_of == s, value, 0.0) for s in range(own_seqs)], axis=1
        )

    def take(h):
        weight = blocks(weight_v[h])
        high = weight.astype(BF16)
        rest = weight - high.astype(F32)
        middle = rest.astype(BF16)
        low = (rest - middle.astype(F32)).astype(BF16)
        values = last_values[:, :, h * HEAD : (h + 1) * HEAD].astype(F32)
        values = values.reshape(own, HEAD).astype(BF16)
        added = lax.dot_general(
            jnp.concatenate([high, middle, low], axis=0),
            jnp.concatenate([values] * 3, axis=0),
            (((0,), (0,)), ((), ())),
            preferred_element_type=F32,
        )
        for s in range(own_seqs):
            column = h * own + s * props
            total = (
                columns[:, column : column + 1] * state_v[s, h]
                + added[s * HEAD : (s + 1) * HEAD]
            )
            taken[s, h] = total
            high, low = split(total)
            t_high[h, s * HEAD : (s + 1) * HEAD, :] = high
            t_low[h, s * HEAD : (s + 1) * HEAD, :] = low

    take_after = [1, 1, 1] + [4, 6] + [half_n] * heads
    take_after = take_after[:heads]
    prepare()
    for step in range(1, half_n + 1):
        if step > 1:
            start_sq(RIGHT, step)
            start_sq(LEFT, step)
            for p in range(PIECES):
                for way in (RIGHT, LEFT):
                    if step > 2 or first_way(p) == way:
                        start_sum(way, step, p)
        for h in range(heads):
            if min(take_after[h], half_n) == step:
                take(h)

    sq_copy(RIGHT, half_n).wait_recv()
    sq_copy(LEFT, half_n).wait_recv()
    square = squares[me]
    for way in (RIGHT, LEFT):
        square = square + sq_in[slot_of(way, half_n, 0, 1)]
    square = jnp.sum(
        jnp.where(
            lax.broadcasted_iota(jnp.int32, (own, 128), 0)
            == lax.broadcasted_iota(jnp.int32, (own, 128), 1),
            square,
            0.0,
        ),
        axis=1,
        keepdims=True,
    )
    row_scale = lax.rsqrt(square / width + EPSILON)

    order = column_order(n)
    place = {slot: i for i, slot in enumerate(order)}
    n_passed = 2 * len(range(2, half_n, 2))

    def all_copy(src_slot, dst_slot, p, offset):
        there = place[dst_slot]
        index = (there - 1) * GROUPS + p if there <= n_passed else n_passed * GROUPS
        return remote(
            gathered.at[place[src_slot], p],
            gathered.at[there, p],
            all_send.at[0],
            all_recv.at[index],
            {"kv": at(offset)},
        )

    def spread_from(slot, p):
        if slot < half_n:
            for offset in (1, 2):
                if slot + offset <= half_n:
                    all_copy(slot, slot + offset, p, offset).start()
        if slot == 0 or slot > half_n:
            back = (n - slot) % n
            for offset in (1, 2):
                if back + offset < half_n:
                    all_copy(slot, n - back - offset, p, -offset).start()

    def head_out(p, j, fin):
        h = p * per_piece + j
        lanes = [slice(x * wide + j * HEAD, x * wide + (j + 1) * HEAD) for x in range(4)]
        floor_gate = lower_bound[pl.ds(core * heads + h, 1), :]
        gain_head = head_gain[pl.ds(core * heads + h, 1), :]
        query = jax.nn.silu(fin[:, lanes[0]]) * HEAD ** (-0.5)
        forget = floor_gate + (1.0 - floor_gate) * jax.nn.sigmoid(fin[:, lanes[1]])
        key = 1.0 - forget
        value = fin[:, lanes[2]]
        gate = jax.nn.silu(fin[:, lanes[3]])
        recurrent = jnp.sum(query * key, axis=1, keepdims=True) * value
        decay = query
        for lag in range(1, props):
            ok = pos >= lag
            decay = decay * jnp.where(pos >= lag - 1, pltpu.roll(forget, lag - 1, 0), 1.0)
            score = jnp.sum(decay * pltpu.roll(key, lag, 0), axis=1, keepdims=True)
            recurrent = recurrent + jnp.where(ok, score, 0.0) * pltpu.roll(value, lag, 0)
        decay = decay * jnp.where(pos >= props - 1, pltpu.roll(forget, props - 1, 0), 1.0)
        high, low = split(blocks(decay))
        carried = jnp.dot(
            jnp.concatenate([high, low], axis=0), t_high[h], preferred_element_type=F32
        )
        recurrent = (
            recurrent
            + carried[:own]
            + carried[own:]
            + jnp.dot(high, t_low[h], preferred_element_type=F32)
        )
        mean = jnp.mean(recurrent * recurrent, axis=1, keepdims=True)
        return (recurrent * lax.rsqrt(mean + EPSILON) * gain_head * gate).astype(BF16)

    for p in range(PIECES):
        sum_copy(RIGHT, half_n, p).wait_recv()
        sum_copy(LEFT, half_n, p).wait_recv()
        fin = (
            product[p, me]
            + sums_in[slot_of(RIGHT, half_n, p, PIECES)].astype(F32)
            + sums_in[slot_of(LEFT, half_n, p, PIECES)].astype(F32)
        ) * row_scale
        for j in range(per_piece):
            column = (p % SUB * per_piece + j) * HEAD
            gathered[0, p // SUB, :, column : column + HEAD] = head_out(p, j, fin)
        if p % SUB == SUB - 1:
            spread_from(0, p // SUB)

    for slot in order[1 : 1 + n_passed]:
        for p in range(GROUPS):
            all_copy(0, slot, p, 1).wait_recv()
            spread_from(slot, p)
    ends = gathered.at[pl.ds(1 + n_passed, n - 1 - n_passed)]
    remote(
        ends, ends, all_send.at[0], all_recv.at[n_passed * GROUPS], {"kv": at(1)}
    ).wait_recv()

    load_wo.wait()
    total = jnp.zeros((rows, wo_v.shape[1]), F32)
    for g in range(GROUPS):
        total = total + jnp.dot(
            gathered[:, g].reshape(rows, SUB * wide),
            wo_v[g * SUB * wide : (g + 1) * SUB * wide, :],
            preferred_element_type=F32,
        )
    out_cols = wo_v.shape[1] // 2
    for c in range(2):
        halves[c] = total[:, c * out_cols : (c + 1) * out_cols].astype(BF16)
    swap = remote(
        halves.at[1 - core], other, half_send.at[0], half_recv.at[0], {"tp": 1 - core}
    )
    swap.start()
    swap.wait_recv()
    result = (halves[core].astype(F32) + other[...].astype(F32)).astype(BF16)
    for slot in range(n):
        mixed[pl.ds(at(-order[slot]) * own, own), :] = result[slot * own : (slot + 1) * own]

    swap.wait_send()
    sent = gathered.at[pl.ds(1, n - 1)]
    remote(sent, sent, all_send.at[0], all_recv.at[0], {"kv": at(1)}).wait_send()
    remote(sums_out, sums_in, sum_send.at[0], sum_recv.at[0], {"kv": at(1)}).wait_send()
    remote(sq_out, sq_in, sq_send.at[0], sq_recv.at[0], {"kv": at(1)}).wait_send()


def per_device(
    tokens,
    w_query,
    w_forget,
    w_input,
    w_gate,
    w_out,
    gain,
    head_gain,
    lower_bound,
    state,
    last_forget,
    last_values,
    accepted,
):
    n = lax.axis_size("kv")
    half_n = n // 2
    seqs, props, feat = tokens.shape
    rows = seqs * props
    own = rows // n
    cols = w_query.shape[1]
    heads = cols // HEAD
    wide = cols // PIECES
    out_cols = w_out.shape[1]
    any_space = pl.BlockSpec(memory_space=pltpu.HBM)
    vmem = pl.BlockSpec(memory_space=pltpu.VMEM)
    dma = pltpu.SemaphoreType.DMA
    inputs = [
        tokens,
        w_query,
        w_forget,
        w_input,
        w_gate,
        w_out,
        gain.reshape(-1, 128),
        head_gain.reshape(-1, 128),
        lower_bound.reshape(-1, 128),
        state,
        last_forget,
        last_values,
        accepted,
    ]
    inputs = [pltpu.with_memory_space_constraint(x, pltpu.HBM) for x in inputs]
    mixed, taken = pl.pallas_call(
        functools.partial(kernel, n),
        out_shape=(
            pltpu.VMEM((rows, out_cols // 2), BF16),
            pltpu.VMEM(state.shape, F32),
        ),
        in_specs=[any_space] * 13,
        out_specs=(vmem, vmem),
        scratch_shapes=[
            pltpu.SMEM(accepted.shape, jnp.int32),
            pltpu.VMEM((gain.size // 128, 128), F32),
            pltpu.VMEM((head_gain.size // 128, 128), F32),
            pltpu.VMEM((lower_bound.size // 128, 128), F32),
            pltpu.VMEM(last_forget.shape, F32),
            pltpu.VMEM(last_values.shape, BF16),
            pltpu.VMEM((seqs, props, feat), BF16),
            pltpu.VMEM((rows, feat), BF16),
            pltpu.VMEM((4, feat, cols), BF16),
            pltpu.VMEM(w_out.shape, BF16),
            pltpu.VMEM(state.shape, F32),
            pltpu.VMEM((heads, own // props * HEAD, HEAD), BF16),
            pltpu.VMEM((heads, own // props * HEAD, HEAD), BF16),
            pltpu.VMEM((heads, own, HEAD), F32),
            pltpu.VMEM((heads * own, HEAD), F32),
            pltpu.VMEM((HEAD, heads * own), F32),
            pltpu.VMEM((PIECES, n, own, 4 * wide), F32),
            pltpu.VMEM((n, 1, 128), F32),
            pltpu.VMEM(((n - 1) * PIECES, own, 4 * wide), BF16),
            pltpu.VMEM(((n - 1) * PIECES, own, 4 * wide), BF16),
            pltpu.VMEM((n - 1, 1, 128), F32),
            pltpu.VMEM((n - 1, 1, 128), F32),
            pltpu.VMEM((n, GROUPS, own, SUB * wide), BF16),
            pltpu.VMEM((2, rows, out_cols // 2), BF16),
            pltpu.VMEM((rows, out_cols // 2), BF16),
            dma((9,)),
            dma((4,)),
            dma((1,)),
            dma(((n - 1) * PIECES,)),
            dma((1,)),
            dma((n - 1,)),
            dma((1,)),
            dma(((len(range(2, half_n, 2)) * 2) * GROUPS + 1,)),
            dma((1,)),
            dma((1,)),
        ],
        compiler_params=pltpu.CompilerParams(
            collective_id=0, has_side_effects=True, vmem_limit_bytes=32 * 1024 * 1024
        ),
    )(*inputs)
    return mixed.reshape(seqs, props, out_cols // 2), taken


def solution(mesh):
    in_specs = (
        P(("grp", "dp"), None, "kv"),
        P("kv", "tp"),
        P("kv", "tp"),
        P("kv", "tp"),
        P("kv", "tp"),
        P("tp", "kv"),
        P(),
        P(),
        P(),
        P(("grp", "dp", "kv"), "tp", None, None),
        P(("grp", "dp", "kv"), None, "tp"),
        P(("grp", "dp", "kv"), None, "tp"),
        P(("grp", "dp", "kv")),
    )
    out_specs = (P(("grp", "dp"), None, ("kv", "tp")), P(("grp", "dp", "kv"), "tp", None, None))
    return jax.shard_map(
        per_device, mesh=mesh, in_specs=in_specs, out_specs=out_specs, check_vma=False
    )
```

time: 102 us -> 95.6 us (0.937)
  Pallas kernels: 96.9 us -> 92.9 us
  local copies, waits for them, and re-layouts: 4.63 us -> 1.95 us
    pallas_call x1, Pallas kernels: 96.9 us -> 92.9 us  [per_device(): pl.pallas_call(functools.partial(kernel, n), out_shape=(pltpu.VMEM((rows,...]
    unnamed x2, local copies, waits for them, and re-layouts: 4.63 us -> 1.95 us
where the time goes in v2:
time: 95.6 us; the launch traced here: 95.5 us
  Pallas kernels  92.9 us (97%)
  local copies, waits for them, and re-layouts  1.95 us (2%)
    pallas_call x1, Pallas kernels, per_device(): pl.pallas_call(functools.partial(kernel, n), out_shape=(pltpu.VMEM((rows,...  92.9 us
    unnamed x2, local copies, waits for them, and re-layouts  1.95 us

profile of v2, /device:TPU:65, one launch (start us, length us, event | category | flops | bytes accessed | tf_op | source)
XLA Modules:
  0.0 95.5 jit_solution(5739399398397365954)
XLA Ops:
  0.6 92.9 %shard_map.140 = (bf16[256,128]{1,0:T(8,128)(2,1)S(1)}, f32[4,8,128,128]{3,2,1,0:T(8,128)S(1)}) custom-call(bf16[64,4,256]{2,1,0:T(4,128)(2,1)} %tokens.1, bf16[256,1024]{1,0:T(8,128)(2,1)} %w_query.1, bf16[256,1024]{1,0:T(8,128)(2,1)} %w_forget.1, bf16[256,1024]{1,0:T(8,128)(2,1)} %w_input.1, bf16[256,1024]{1,0:T(8,128)(2,1)} %w_gate.1, ...), custom_call_target="tpu_custom_call" | custom-call | tf_op jit(solution)/shard_map/pallas_call | solution.py:472
  93.5 0.6 copy.17
  94.2 1.3 %copy.18 = f32[4,8,128,128]{3,2,1,0:T(8,128)} copy(f32[4,8,128,128]{3,2,1,0:T(8,128)S(1)} %get-tuple-element.7) | data formatting | bytes 4194304
